TPU v7x, 32 devices: a whole 2x2x4 slice. The times are simulated.
32 devices in a mesh: fs: 8 (over z, y), tp: 4 (over x, core).
Axes of the slice: x: 2, y: 2, z: 4, core: 2. Of those that a mesh axis runs over, the one named last changes fastest.
Arguments:
- tokens: bfloat16 [3072, 2048], P('tp'), may hold values from -6 to 6
- norm_gain: float32 [2048], P('fs'), may hold values from 0.1 to 1.9
- gate_weight: float32 [4, 2048, 8192], P(None, 'fs', 'tp'), may hold values from -0.125 to 0.125
- up_weight: float32 [4, 2048, 8192], P(None, 'fs', 'tp'), may hold values from -0.125 to 0.125
- down_weight: float32 [4, 8192, 2048], P(None, 'fs', 'tp'), may hold values from -0.0625 to 0.0625
- routes: int32 [3072, 2], P('tp'), may hold values from 0 to 3, all different within a row; in each aligned block of 768 rows (0 to 767, 768 to 1535, ...) at most 480 rows name the same one
- route_logit: float32 [3072, 2], P('tp'), may hold values from -6 to 6
Outputs:
- gate_out: bfloat16 [4, 2048, 8192], P(None, None, 'fs')
- up_out: bfloat16 [4, 2048, 8192], P(None, None, 'fs')
- down_out: bfloat16 [4, 8192, 2048], P(None, 'fs')
- mixed: bfloat16 [3072, 2048], P(('tp', 'fs'))
Inputs may be any that keep to these rules, and one draw needn't show every extreme that they name: `routes`: the two experts of a token differ. In each aligned block of 768 tokens (the tokens of one request group) every expert is named by at most 480 tokens, a bound that some block reaches.
All inputs are finite; a program needn't handle non-finite values.
Results may differ from a plain program's by a relative error of at most 0.0082.
Values may be sent and summed in bfloat16 or wider, within the bound.
No kernel may reach another device: no remote copies, remote signals or barrier semaphores. Data moves between devices by JAX's collectives and lax.ppermute only.
A program may use at most 192 MiB of HBM per device.

v0:
```python
import jax
import jax.numpy as jnp
from jax import lax
from jax.sharding import PartitionSpec as P

EPS = 0.5


def shards(tokens, norm_gain, gate_weight, up_weight, down_weight, routes, route_logit):
    gain_col = norm_gain[None, :, None]
    gate_part = (gate_weight * gain_col).astype(jnp.bfloat16)
    up_part = (up_weight * gain_col).astype(jnp.bfloat16)
    down_part = down_weight.astype(jnp.bfloat16)
    gate_one, up_one = (
        lax.all_to_all(gate_part, "tp", split_axis=0, concat_axis=2, tiled=True),
        lax.all_to_all(up_part, "tp", split_axis=0, concat_axis=2, tiled=True),
    )
    gate_mine, up_mine = (
        lax.all_to_all(gate_one, "fs", split_axis=2, concat_axis=1, tiled=True),
        lax.all_to_all(up_one, "fs", split_axis=2, concat_axis=1, tiled=True),
    )
    gate_out, up_out = (
        lax.all_gather(gate_mine, "tp", axis=0, tiled=True),
        lax.all_gather(up_mine, "tp", axis=0, tiled=True),
    )
    down_out = lax.all_gather(down_part, "tp", axis=2, tiled=True)
    total_rows = tokens.shape[0]
    width = tokens.shape[1]
    experts = gate_out.shape[0]
    capacity = total_rows * 5 // 8
    floats = tokens.astype(jnp.float32)
    normed = (floats * lax.rsqrt(jnp.mean(floats * floats, axis=1, keepdims=True) + EPS)).astype(
        jnp.bfloat16
    )
    first_share = jax.nn.sigmoid(route_logit[:, 0] - route_logit[:, 1])
    shares = jnp.stack([first_share, 1.0 - first_share], axis=1)
    chosen = (routes[:, :, None] == jnp.arange(experts, dtype=jnp.int32)[None, None, :]).astype(
        jnp.int32
    )
    counts = jnp.sum(chosen, axis=1)
    before = jnp.cumsum(counts, axis=0) - counts
    slot_index = jnp.sum(chosen * before[:, None, :], axis=2)
    flat_slot = routes * capacity + slot_index
    row_ids = jnp.repeat(jnp.arange(total_rows, dtype=jnp.int32), 2)
    table = (
        jnp.full((experts * capacity,), total_rows, jnp.int32)
        .at[flat_slot.reshape(-1)]
        .set(row_ids)
    )
    gathered = jnp.take(normed, table, axis=0, mode="fill", fill_value=0).reshape(
        experts, capacity, width
    )
    gate_val = jnp.einsum("ecd,edf->ecf", gathered, gate_out, preferred_element_type=jnp.float32)
    up_val = jnp.einsum("ecd,edf->ecf", gathered, up_out, preferred_element_type=jnp.float32)
    hidden = (jax.nn.silu(gate_val) * up_val).astype(jnp.bfloat16)
    results = jnp.einsum("ecf,efd->ecd", hidden, down_out, preferred_element_type=jnp.float32)
    flat_rows = results.reshape(experts * capacity, width)
    first_rows = jnp.take(flat_rows, flat_slot[:, 0], axis=0)
    second_rows = jnp.take(flat_rows, flat_slot[:, 1], axis=0)
    mixed = lax.psum_scatter(
        shares[:, 0:1] * first_rows + shares[:, 1:2] * second_rows,
        "fs",
        scatter_dimension=0,
        tiled=True,
    )
    return (gate_out, up_out, down_out, mixed.astype(jnp.bfloat16))


def solution(mesh):
    return jax.shard_map(
        shards,
        mesh=mesh,
        in_specs=(
            P("tp", None),
            P("fs"),
            P(None, "fs", "tp"),
            P(None, "fs", "tp"),
            P(None, "fs", "tp"),
            P("tp", None),
            P("tp", None),
        ),
        out_specs=(
            P(None, None, "fs"),
            P(None, None, "fs"),
            P(None, "fs", None),
            P(("tp", "fs"), None),
        ),
        check_vma=False,
    )
```

profile of v0, /device:TPU:0, one launch (start us, length us, event | category | flops | bytes accessed | tf_op | source)
XLA Modules:
  0.0 959.0 jit_solution(9687158230475078291)
XLA Ops:
  7.2 8.7 copy.43
  15.9 8.7 copy.46
  24.6 10.7 %multiply_convert_fusion = (bf16[4,256,2048]{1,2,0:T(8,128)(2,1)}, bf16[4,256,2048]{1,2,0:T(8,128)(2,1)}) fusion(f32[4,256,2048]{1,2,0:T(8,128)} %copy.46, f32[256]{0:T(256)S(1)} %copy-done.3, f32[4,256,2048]{1,2,0:T(8,128)} %copy.43), kind=kLoop, calls=%fused_computation.4 | loop fusion | flops 8388608 | bytes 25166848 | tf_op jit(solution)/shard_map/convert_element_type | solution.py:12
  35.3 52.6 %all_to_all.72 = bf16[4,256,2048]{1,2,0:T(8,128)(2,1)S(1)} all-to-all(bf16[4,256,2048]{1,2,0:T(8,128)(2,1)} %get-tuple-element.9), channel_id=1, replica_groups=mesh['fs'=8,'tp'=4] {'tp'}, dimensions={0} | all-to-all | bytes 8388608 | tf_op jit(solution)/shard_map/all_to_all | solution.py:16
  87.9 49.3 %copy.56 = bf16[1,256,8192]{1,0,2:T(2,128)(2,1)} copy(bf16[1,256,8192]{1,2,0:T(8,128)(2,1)S(1)} %bitcast.49) | data formatting | bytes 8388608 | tf_op jit(solution)/shard_map/all_to_all | solution.py:16
  137.7 43.5 %reduce.13 = bf16[8192,256]{1,0:T(8,128)(2,1)} reduce(bf16[8192,1,256]{2,1,0:T(2,128)(2,1)} %bitcast.45, bf16[]{:T(256)} %broadcast.78), dimensions={1}, to_apply=%bitcast.40.reduce_sub_computation | reduce | bytes 8388610
  181.2 6.9 reshape.137
  188.2 99.8 %all_to_all.73 = bf16[8,2,131072]{2,1,0:T(2,128)(2,1)} all-to-all(bf16[8,2,131072]{2,1,0:T(2,128)(2,1)} %reshape.137), channel_id=1, replica_groups=mesh['fs'=8,'tp'=4] {'fs'}, dimensions={0} | all-to-all | bytes 8388608 | tf_op jit(solution)/shard_map/all_to_all | solution.py:20
  288.0 8.7 reshape.138
  296.7 6.1 copy.51
  302.8 6.4 copy.48
  309.3 6.0 convert_element_type.26
  315.4 97.4 %all_to_all.74 = bf16[4,256,2048]{1,2,0:T(8,128)(2,1)S(1)} all-to-all(bf16[4,256,2048]{1,2,0:T(8,128)(2,1)} %get-tuple-element.10), channel_id=1, replica_groups=mesh['fs'=8,'tp'=4] {'tp'}, dimensions={0} | all-to-all | bytes 8388608 | tf_op jit(solution)/shard_map/all_to_all | solution.py:15
  412.8 49.3 %copy.57 = bf16[1,256,8192]{1,0,2:T(2,128)(2,1)} copy(bf16[1,256,8192]{1,2,0:T(8,128)(2,1)S(1)} %bitcast.51) | data formatting | bytes 8388608 | tf_op jit(solution)/shard_map/all_to_all | solution.py:15
  462.2 43.5 %reduce.12 = bf16[8192,256]{1,0:T(8,128)(2,1)} reduce(bf16[8192,1,256]{2,1,0:T(2,128)(2,1)} %bitcast.46, bf16[]{:T(256)} %broadcast.78), dimensions={1}, to_apply=%bitcast.41.reduce_sub_computation | reduce | bytes 8388610
  505.7 7.0 reshape.135
  512.7 97.7 %all_to_all.75 = bf16[8,2,131072]{2,1,0:T(2,128)(2,1)} all-to-all(bf16[8,2,131072]{2,1,0:T(2,128)(2,1)} %reshape.135), channel_id=1, replica_groups=mesh['fs'=8,'tp'=4] {'fs'}, dimensions={0} | all-to-all | bytes 8388608 | tf_op jit(solution)/shard_map/all_to_all | solution.py:19
  610.4 8.7 reshape.136
  619.1 6.1 copy.50
  625.2 6.6 copy.45
  634.9 6.3 scatter_custom_fusion
  644.9 8.9 gather_fusion
  654.0 16.3 %fusion = f32[4,480,1024]{2,1,0:T(8,128)} fusion(bf16[4,2048,1024]{2,1,0:T(8,128)(2,1)} %all-gather.6.cloned.1.call-done, bf16[4,480,2048]{2,1,0:T(8,128)(2,1)} %bitcast.57, pred[4,480]{1,0:T(4,128)(4,1)S(1)} %broadcast_in_dim.37), kind=kOutput, calls=%fused_computation.10 | convolution fusion | flops 8056995840 | bytes 32507776 | tf_op jit(solution)/shard_map/ecd,edf->ecf/dot_general | solution.py:54
  670.2 65.7 %all-gather.4.cloned.1.call-done = bf16[4,2048,1024]{2,1,0:T(8,128)(2,1)} async-done(((bf16[1,2048,1024]{2,1,0:T(8,128)(2,1)}), bf16[4,2048,1024]{2,1,0:T(8,128)(2,1)}) %all-gather.4.cloned.1.call-update) | async-done | bytes 16777232 | tf_op jit(solution)/shard_map/all_gather | solution.py:23
  735.9 27.2 %fusion.7 = f32[4,480,2048]{2,1,0:T(8,128)} fusion(bf16[4,1024,2048]{2,1,0:T(8,128)(2,1)} %all-gather.8.cloned.1.call-done, f32[4,480,1024]{2,1,0:T(8,128)} %fusion, bf16[4,2048,1024]{2,1,0:T(8,128)(2,1)} %all-gather.4.cloned.1.call-done, bf16[4,480,2048]{2,1,0:T(8,128)(2,1)} %bitcast.58, pred[4,480]{1,0:T(4,128)(4,1)S(1)} %broadcast_in_dim.37), kind=kOutput, calls=%fused_computation.19 | convolution fusion | flops 16121856000 | bytes 65013632 | tf_op jit(solution)/shard_map/ecf,efd->ecd/dot_general | solution.py:56
  763.1 12.7 %gather_fusion.1 = f32[768,2048]{1,0:T(8,128)} fusion(f32[1920,2048]{1,0:T(8,128)} %bitcast.43, s32[1024]{0:T(1024)S(1)} %pad_clamp_fusion.2), kind=kCustom, calls=%fused_computation.clone | custom fusion | bytes 12585984 | tf_op jit(solution)/shard_map/jit(_take)/gather | solution.py:58
  775.8 12.7 %gather_fusion.2 = f32[768,2048]{1,0:T(8,128)} fusion(f32[1920,2048]{1,0:T(8,128)} %bitcast.44, s32[1024]{0:T(1024)S(1)} %pad_clamp_fusion.1), kind=kCustom, calls=%fused_computation.1.clone | custom fusion | bytes 12585984 | tf_op jit(solution)/shard_map/jit(_take)/gather | solution.py:59
  788.5 7.2 fusion.4
  795.7 118.2 %reduce-scatter.2.cloned.1.call-done = f32[96,2048]{1,0:T(8,128)} async-done(((f32[768,2048]{1,0:T(8,128)}), f32[96,2048]{1,0:T(8,128)}) %reduce-scatter.2.cloned.1.call-update) | async-done | bytes 786448 | tf_op jit(solution)/shard_map/reduce_scatter | solution.py:60
  915.8 15.2 %copy.61 = bf16[4,2048,1024]{2,1,0:T(8,128)(2,1)} copy(bf16[4,2048,1024]{2,1,0:T(8,128)(2,1)} %all-gather.4.cloned.1.call-done) | data formatting | bytes 33554432
  931.1 15.2 %copy.62 = bf16[4,2048,1024]{2,1,0:T(8,128)(2,1)} copy(bf16[4,2048,1024]{2,1,0:T(8,128)(2,1)} %all-gather.6.cloned.1.call-done) | data formatting | bytes 33554432
  946.3 6.2 copy.63
  (56 shorter events, 9.4 us)
Async XLA Ops:
  7.2 646.8 %all-gather.6.cloned.1.call-start = ((), (), s32[]{:S(2)}) async-start(), calls=%async_computation.6 | async-start | bytes 20971520 | tf_op jit(solution)/shard_map/all_gather | solution.py:24
  15.9 8.7 copy-start.3
  309.3 360.9 %all-gather.8.cloned.1.call-start = ((), (), s32[]{:S(2)}) async-start(), calls=%async_computation.7 | async-start | bytes 20971520 | tf_op jit(solution)/shard_map/all_gather | solution.py:26
  315.4 420.5 %all-gather.4.cloned.1.call-start = ((), (), s32[]{:S(2)}) async-start(), calls=%async_computation.5 | async-start | bytes 20971520 | tf_op jit(solution)/shard_map/all_gather | solution.py:23
  625.2 6.7 copy-start.1
  625.2 16.2 %copy-start = (bf16[768,2048]{1,0:T(8,128)(2,1)S(1)}, bf16[768,2048]{1,0:T(8,128)(2,1)}, u32[]{:S(2)}) copy-start(bf16[768,2048]{1,0:T(8,128)(2,1)} %param.9) | copy-start | bytes 9437188
  631.8 282.1 %reduce-scatter.2.cloned.1.call-start = ((), (), s32[]{:S(2)}) async-start(), calls=%async_computation.8 | async-start | bytes 7077888 | tf_op jit(solution)/shard_map/reduce_scatter | solution.py:60
  644.9 8.9 copy-start.2
  915.8 30.5 %slice-start = ((s8[16777216]{0:T(1024)(128)(4,1)}), s8[4194304]{0:T(1024)(128)(4,1)S(1)}, s32[]{:S(2)}) async-start(s8[16777216]{0:T(1024)(128)(4,1)} %bitcast.53), calls=%async_computation.9 | async-start | bytes 8388608
  915.8 30.5 %slice-start.1 = ((s8[16777216]{0:T(1024)(128)(4,1)}), s8[4194304]{0:T(1024)(128)(4,1)S(1)}, s32[]{:S(2)}) async-start(s8[16777216]{0:T(1024)(128)(4,1)} %bitcast.53), calls=%async_computation.10 | async-start | bytes 8388608
  931.1 15.2 %slice-start.2 = ((s8[16777216]{0:T(1024)(128)(4,1)}), s8[4194304]{0:T(1024)(128)(4,1)S(1)}, s32[]{:S(2)}) async-start(s8[16777216]{0:T(1024)(128)(4,1)} %bitcast.53), calls=%async_computation.11 | async-start | bytes 8388608
  931.1 15.2 %slice-start.3 = ((s8[16777216]{0:T(1024)(128)(4,1)}), s8[4194304]{0:T(1024)(128)(4,1)S(1)}, s32[]{:S(2)}) async-start(s8[16777216]{0:T(1024)(128)(4,1)} %bitcast.53), calls=%async_computation.12 | async-start | bytes 8388608
Sparse Core Ops, SparseCore 0:
  309.4 148.9 all-gather.5
  460.0 104.8 all-gather.7
  631.9 103.9 all-gather.3
  795.8 118.0 reduce-scatter.1
where the time goes:
time: 961 us; the launch traced here: 959 us
  blocking collectives  347 us (36%)
  local copies, waits for them, and re-layouts  252 us (26%)
  waiting for transfers between devices  184 us (19%)
  other arithmetic  118 us (12%)
  matrix products  43.5 us (5%)
  between operations  14 us (1%)
    reduce_scatter x1, waiting for transfers between devices, shards(): lax.psum_scatter(shares[:, 0:1] * first_rows + shares[:, 1:2] * second_ro...  118 us
    all_to_all x1, blocking collectives, shards(): lax.all_to_all(up_one, 'fs', split_axis=2, concat_axis=1, tiled=True)  99.8 us
    unnamed x28, local copies, waits for them, and re-layouts  98.2 us
    all_to_all x1, blocking collectives, shards(): lax.all_to_all(gate_one, 'fs', split_axis=2, concat_axis=1, tiled=True)  97.7 us
    all_to_all x1, blocking collectives, shards(): lax.all_to_all(gate_part, 'tp', split_axis=0, concat_axis=2, tiled=True)  97.4 us
    unnamed x4, other arithmetic  87.2 us
    all_gather x1, waiting for transfers between devices, shards(): lax.all_gather(gate_mine, 'tp', axis=0, tiled=True)  65.7 us
    all_to_all x1, blocking collectives, shards(): lax.all_to_all(up_part, 'tp', split_axis=0, concat_axis=2, tiled=True)  52.6 us
  transfers between devices with their start and end apart: 4, of which 2 were waited for; matrix products, arithmetic and copies ran while one was open for 17% of the time, Pallas kernels for 0%

commit v1 on v0

--- a/solution.py
+++ b/solution.py
@@ -4,6 +4,35 @@
 from jax.sharding import PartitionSpec as P
 
 EPS = 0.5
+
+
+def _define_patches(in_array, axis_no, local):
+    local_out = in_array.shape
+    near = in_array.reshape(
+        *local_out[:axis_no], local, local_out[axis_no] // local, *local_out[axis_no + 1 :]
+    )
+    return jnp.moveaxis(near, axis_no, 0)
+
+
+def close_ladders(page, join_dim):
+    seen_now = list(page.shape[1:])
+    seen_now[join_dim] *= page.shape[0]
+    return jnp.moveaxis(page, 0, join_dim).reshape(seen_now)
+
+
+def _move_columns(patch, block_in, bus_axis, panel):
+    view_out = lax.axis_size(bus_axis)
+    tmp, q_next = (view_out, lax.axis_index(bus_axis))
+    moved = _define_patches(patch, panel, tmp)
+    grid = [moved[q_next]]
+    i0 = 1
+    while i0 < tmp:
+        state_now = moved[q_next ^ i0]
+        grid.append(lax.ppermute(state_now, bus_axis, [(to_i, to_i ^ i0) for to_i in range(tmp)]))
+        i0 += 1
+    e_now = jnp.stack(grid, axis=0)
+    moved = e_now[q_next ^ jnp.arange(tmp)]
+    return close_ladders(moved, block_in)
 
 
 def shards(tokens, norm_gain, gate_weight, up_weight, down_weight, routes, route_logit):
@@ -13,7 +42,7 @@
     down_part = down_weight.astype(jnp.bfloat16)
     gate_one, up_one = (
         lax.all_to_all(gate_part, "tp", split_axis=0, concat_axis=2, tiled=True),
-        lax.all_to_all(up_part, "tp", split_axis=0, concat_axis=2, tiled=True),
+        _move_columns(up_part, 2, "tp", 0),
     )
     gate_mine, up_mine = (
         lax.all_to_all(gate_one, "fs", split_axis=2, concat_axis=1, tiled=True),

time: 961 us -> 926 us (0.964)
  blocking collectives: 347 us -> 295 us
  waiting for transfers between devices: 184 us -> 230 us
  local copies, waits for them, and re-layouts: 252 us -> 219 us
    all_to_all x1 -> x0, blocking collectives: 52.6 us -> none  [shards(): lax.all_to_all(up_part, 'tp', split_axis=0, concat_axis=2, tiled=True)]
    all_to_all x1 -> x0, local copies, waits for them, and re-layouts: 49.3 us -> none  [shards(): lax.all_to_all(up_part, 'tp', split_axis=0, concat_axis=2, tiled=True)]
    ppermute x0 -> x3, waiting for transfers between devices: none -> 45.9 us  [_move_columns(): lax.ppermute(state_now, bus_axis, [(to_i, to_i ^ i0) for to_i in range(tm...]
  transfers between devices with their start and end apart: 4 -> 7, of which waited for: 2 -> 4; matrix products, arithmetic and copies ran while one was open for 17% -> 18% of each run, Pallas kernels for 0% -> 0%
where the time goes in v1:
time: 926 us; the launch traced here: 924 us
  blocking collectives  295 us (32%)
  waiting for transfers between devices  230 us (25%)
  local copies, waits for them, and re-layouts  219 us (24%)
  other arithmetic  120 us (13%)
  matrix products  43.5 us (5%)
  between operations  14 us (2%)
    reduce_scatter x1, waiting for transfers between devices, shards(): lax.psum_scatter(shares[:, 0:1] * first_rows + shares[:, 1:2] * second_ro...  118 us
    all_to_all x1, blocking collectives, shards(): lax.all_to_all(up_one, 'fs', split_axis=2, concat_axis=1, tiled=True)  99.6 us
    unnamed x28, local copies, waits for them, and re-layouts  98.1 us
    all_to_all x1, blocking collectives, shards(): lax.all_to_all(gate_one, 'fs', split_axis=2, concat_axis=1, tiled=True)  97.8 us
    all_to_all x1, blocking collectives, shards(): lax.all_to_all(gate_part, 'tp', split_axis=0, concat_axis=2, tiled=True)  97.2 us
    unnamed x4, other arithmetic  87.2 us
    all_gather x1, waiting for transfers between devices, shards(): lax.all_gather(gate_mine, 'tp', axis=0, tiled=True)  65.7 us
    all_to_all x1, local copies, waits for them, and re-layouts, shards(): lax.all_to_all(gate_part, 'tp', split_axis=0, concat_axis=2, tiled=True)  49.3 us
  transfers between devices with their start and end apart: 7, of which 4 were waited for; matrix products, arithmetic and copies ran while one was open for 18% of the time, Pallas kernels for 0%

profile of v1, /device:TPU:0, one launch (start us, length us, event | category | flops | bytes accessed | tf_op | source)
XLA Modules:
  0.0 924.2 jit_solution(3058394377603839443)
XLA Ops:
  7.2 8.7 copy.43
  15.9 8.7 copy.46
  24.6 10.7 %multiply_convert_fusion = (bf16[4,256,2048]{1,2,0:T(8,128)(2,1)}, bf16[4,256,2048]{1,2,0:T(8,128)(2,1)}) fusion(f32[4,256,2048]{1,2,0:T(8,128)} %copy.46, f32[256]{0:T(256)S(1)} %copy-done.3, f32[4,256,2048]{1,2,0:T(8,128)} %copy.43), kind=kLoop, calls=%fused_computation.5 | loop fusion | flops 8388608 | bytes 25166848 | tf_op jit(solution)/shard_map/convert_element_type | solution.py:41
  40.9 23.9 %collective-permute-done.1 = bf16[1,256,2048]{1,2,0:T(8,128)(2,1)S(1)} collective-permute-done((bf16[1,256,2048]{1,2,0:T(8,128)(2,1)S(1)}, bf16[1,256,2048]{1,2,0:T(8,128)(2,1)S(1)}, u32[]{:S(2)}, u32[]{:S(2)}) %collective-permute-start.1) | collective-permute-done | bytes 1048608 | tf_op jit(solution)/shard_map/ppermute | solution.py:31
  64.9 21.9 %collective-permute-done.2 = bf16[1,256,2048]{1,2,0:T(8,128)(2,1)S(1)} collective-permute-done((bf16[1,256,2048]{1,2,0:T(8,128)(2,1)S(1)}, bf16[1,256,2048]{1,2,0:T(8,128)(2,1)S(1)}, u32[]{:S(2)}, u32[]{:S(2)}) %collective-permute-start.2) | collective-permute-done | bytes 1048608 | tf_op jit(solution)/shard_map/ppermute | solution.py:31
  94.1 8.6 copy.56
  103.2 43.5 %reduce.13 = bf16[8192,256]{1,0:T(8,128)(2,1)} reduce(bf16[8192,1,256]{2,1,0:T(2,128)(2,1)} %bitcast.54, bf16[]{:T(256)} %broadcast.113), dimensions={1}, to_apply=%bitcast.49.reduce_sub_computation | reduce | bytes 8388610
  146.8 6.9 reshape.175
  153.7 99.6 %all_to_all.54 = bf16[8,2,131072]{2,1,0:T(2,128)(2,1)} all-to-all(bf16[8,2,131072]{2,1,0:T(2,128)(2,1)} %reshape.175), channel_id=1, replica_groups=mesh['fs'=8,'tp'=4] {'fs'}, dimensions={0} | all-to-all | bytes 8388608 | tf_op jit(solution)/shard_map/all_to_all | solution.py:49
  253.3 8.7 reshape.176
  262.0 6.1 copy.51
  268.1 6.4 copy.48
  280.7 97.2 %all_to_all.55 = bf16[4,256,2048]{1,2,0:T(8,128)(2,1)S(1)} all-to-all(bf16[4,256,2048]{1,2,0:T(8,128)(2,1)} %get-tuple-element.14), channel_id=1, replica_groups=mesh['fs'=8,'tp'=4] {'tp'}, dimensions={0} | all-to-all | bytes 8388608 | tf_op jit(solution)/shard_map/all_to_all | solution.py:44
  377.9 49.3 %copy.57 = bf16[1,256,8192]{1,0,2:T(2,128)(2,1)} copy(bf16[1,256,8192]{1,2,0:T(8,128)(2,1)S(1)} %bitcast.60) | data formatting | bytes 8388608 | tf_op jit(solution)/shard_map/all_to_all | solution.py:44
  427.3 43.5 %reduce.12 = bf16[8192,256]{1,0:T(8,128)(2,1)} reduce(bf16[8192,1,256]{2,1,0:T(2,128)(2,1)} %bitcast.55, bf16[]{:T(256)} %broadcast.113), dimensions={1}, to_apply=%bitcast.50.reduce_sub_computation | reduce | bytes 8388610
  470.8 6.9 reshape.173
  477.8 97.8 %all_to_all.56 = bf16[8,2,131072]{2,1,0:T(2,128)(2,1)} all-to-all(bf16[8,2,131072]{2,1,0:T(2,128)(2,1)} %reshape.173), channel_id=1, replica_groups=mesh['fs'=8,'tp'=4] {'fs'}, dimensions={0} | all-to-all | bytes 8388608 | tf_op jit(solution)/shard_map/all_to_all | solution.py:48
  575.6 8.7 reshape.174
  584.3 6.1 copy.50
  590.4 6.6 copy.45
  600.1 6.3 scatter_custom_fusion
  610.1 8.9 gather_fusion.1
  619.2 16.3 %fusion = f32[4,480,1024]{2,1,0:T(8,128)} fusion(bf16[4,2048,1024]{2,1,0:T(8,128)(2,1)} %all-gather.6.cloned.1.call-done, bf16[4,480,2048]{2,1,0:T(8,128)(2,1)} %bitcast.66, pred[4,480]{1,0:T(4,128)(4,1)S(1)} %broadcast_in_dim.38), kind=kOutput, calls=%fused_computation.11 | convolution fusion | flops 8056995840 | bytes 32507776 | tf_op jit(solution)/shard_map/ecd,edf->ecf/dot_general | solution.py:83
  635.5 65.7 %all-gather.4.cloned.1.call-done = bf16[4,2048,1024]{2,1,0:T(8,128)(2,1)} async-done(((bf16[1,2048,1024]{2,1,0:T(8,128)(2,1)}), bf16[4,2048,1024]{2,1,0:T(8,128)(2,1)}) %all-gather.4.cloned.1.call-update) | async-done | bytes 16777232 | tf_op jit(solution)/shard_map/all_gather | solution.py:52
  701.2 27.2 %fusion.7 = f32[4,480,2048]{2,1,0:T(8,128)} fusion(bf16[4,1024,2048]{2,1,0:T(8,128)(2,1)} %all-gather.8.cloned.1.call-done, f32[4,480,1024]{2,1,0:T(8,128)} %fusion, bf16[4,2048,1024]{2,1,0:T(8,128)(2,1)} %all-gather.4.cloned.1.call-done, bf16[4,480,2048]{2,1,0:T(8,128)(2,1)} %bitcast.67, pred[4,480]{1,0:T(4,128)(4,1)S(1)} %broadcast_in_dim.38), kind=kOutput, calls=%fused_computation.21 | convolution fusion | flops 16121856000 | bytes 65013632 | tf_op jit(solution)/shard_map/ecf,efd->ecd/dot_general | solution.py:85
  728.4 12.7 %gather_fusion.2 = f32[768,2048]{1,0:T(8,128)} fusion(f32[1920,2048]{1,0:T(8,128)} %bitcast.52, s32[1024]{0:T(1024)S(1)} %pad_clamp_fusion.2), kind=kCustom, calls=%fused_computation.clone | custom fusion | bytes 12585984 | tf_op jit(solution)/shard_map/jit(_take)/gather | solution.py:87
  741.1 12.7 %gather_fusion.3 = f32[768,2048]{1,0:T(8,128)} fusion(f32[1920,2048]{1,0:T(8,128)} %bitcast.53, s32[1024]{0:T(1024)S(1)} %pad_clamp_fusion.1), kind=kCustom, calls=%fused_computation.1.clone | custom fusion | bytes 12585984 | tf_op jit(solution)/shard_map/jit(_take)/gather | solution.py:88
  753.7 7.2 fusion.4
  761.0 118.1 %reduce-scatter.2.cloned.1.call-done = f32[96,2048]{1,0:T(8,128)} async-done(((f32[768,2048]{1,0:T(8,128)}), f32[96,2048]{1,0:T(8,128)}) %reduce-scatter.2.cloned.1.call-update) | async-done | bytes 786448 | tf_op jit(solution)/shard_map/reduce_scatter | solution.py:89
  881.1 15.2 %copy.61 = bf16[4,2048,1024]{2,1,0:T(8,128)(2,1)} copy(bf16[4,2048,1024]{2,1,0:T(8,128)(2,1)} %all-gather.4.cloned.1.call-done) | data formatting | bytes 33554432
  896.3 15.2 %copy.62 = bf16[4,2048,1024]{2,1,0:T(8,128)(2,1)} copy(bf16[4,2048,1024]{2,1,0:T(8,128)(2,1)} %all-gather.6.cloned.1.call-done) | data formatting | bytes 33554432
  911.5 6.2 copy.63
  (66 shorter events, 28.4 us)
Async XLA Ops:
  7.2 612.0 %all-gather.6.cloned.1.call-start = ((), (), s32[]{:S(2)}) async-start(), calls=%async_computation.5 | async-start | bytes 20971520 | tf_op jit(solution)/shard_map/all_gather | solution.py:53
  15.9 8.7 copy-start.3
  37.8 3.2 collective-permute-start
  38.3 26.6 %collective-permute-start.1 = (bf16[1,256,2048]{1,2,0:T(8,128)(2,1)S(1)}, bf16[1,256,2048]{1,2,0:T(8,128)(2,1)S(1)}, u32[]{:S(2)}, u32[]{:S(2)}) collective-permute-start(bf16[1,256,2048]{1,2,0:T(8,128)(2,1)S(1)} %get-tuple-element.11), channel_id=1, source_target_pairs={{0,2},{1,3},{2,0},{3,1},{4,6},{5,7},{6,4},{7,5},{8,10},{9,11},{10,... | collective-permute-start | bytes 3145736 | tf_op jit(solution)/shard_map/ppermute | solution.py:31
  40.9 46.0 %collective-permute-start.2 = (bf16[1,256,2048]{1,2,0:T(8,128)(2,1)S(1)}, bf16[1,256,2048]{1,2,0:T(8,128)(2,1)S(1)}, u32[]{:S(2)}, u32[]{:S(2)}) collective-permute-start(bf16[1,256,2048]{1,2,0:T(8,128)(2,1)S(1)} %get-tuple-element.10), channel_id=1, source_target_pairs={{0,3},{1,2},{2,1},{3,0},{4,7},{5,6},{6,5},{7,4},{8,11},{9,10},{10,... | collective-permute-start | bytes 3145736 | tf_op jit(solution)/shard_map/ppermute | solution.py:31
  274.6 360.9 %all-gather.8.cloned.1.call-start = ((), (), s32[]{:S(2)}) async-start(), calls=%async_computation.6 | async-start | bytes 20971520 | tf_op jit(solution)/shard_map/all_gather | solution.py:55
  280.7 420.5 %all-gather.4.cloned.1.call-start = ((), (), s32[]{:S(2)}) async-start(), calls=%async_computation.4 | async-start | bytes 20971520 | tf_op jit(solution)/shard_map/all_gather | solution.py:52
  590.4 6.7 copy-start.1
  590.4 16.2 %copy-start = (bf16[768,2048]{1,0:T(8,128)(2,1)S(1)}, bf16[768,2048]{1,0:T(8,128)(2,1)}, u32[]{:S(2)}) copy-start(bf16[768,2048]{1,0:T(8,128)(2,1)} %param.9) | copy-start | bytes 9437188
  597.0 282.1 %reduce-scatter.2.cloned.1.call-start = ((), (), s32[]{:S(2)}) async-start(), calls=%async_computation.7 | async-start | bytes 7077888 | tf_op jit(solution)/shard_map/reduce_scatter | solution.py:89
  610.1 8.9 copy-start.2
  881.1 30.5 %slice-start = ((s8[16777216]{0:T(1024)(128)(4,1)}), s8[4194304]{0:T(1024)(128)(4,1)S(1)}, s32[]{:S(2)}) async-start(s8[16777216]{0:T(1024)(128)(4,1)} %bitcast.62), calls=%async_computation.8 | async-start | bytes 8388608
  881.1 30.5 %slice-start.1 = ((s8[16777216]{0:T(1024)(128)(4,1)}), s8[4194304]{0:T(1024)(128)(4,1)S(1)}, s32[]{:S(2)}) async-start(s8[16777216]{0:T(1024)(128)(4,1)} %bitcast.62), calls=%async_computation.9 | async-start | bytes 8388608
  896.3 15.2 %slice-start.2 = ((s8[16777216]{0:T(1024)(128)(4,1)}), s8[4194304]{0:T(1024)(128)(4,1)S(1)}, s32[]{:S(2)}) async-start(s8[16777216]{0:T(1024)(128)(4,1)} %bitcast.62), calls=%async_computation.10 | async-start | bytes 8388608
  896.3 15.2 %slice-start.3 = ((s8[16777216]{0:T(1024)(128)(4,1)}), s8[4194304]{0:T(1024)(128)(4,1)S(1)}, s32[]{:S(2)}) async-start(s8[16777216]{0:T(1024)(128)(4,1)} %bitcast.62), calls=%async_computation.11 | async-start | bytes 8388608
Sparse Core Ops, SparseCore 0:
  274.7 149.8 all-gather.5
  426.2 104.1 all-gather.7
  597.1 104.0 all-gather.3
  761.1 117.9 reduce-scatter.1
